TPU v7x, 32 devices: a whole 2x2x4 slice. The times are simulated.
32 devices in a mesh: sp: 8 (over z, y), tp: 4 (over x, core).
Axes of the slice: x: 2, y: 2, z: 4, core: 2. Of those that a mesh axis runs over, the one named last changes fastest.
Arguments:
- activity: bfloat16 [2048, 4096], P('sp', 'tp'), may hold values from -8 to 8
- query_weight: bfloat16 [4096, 3072], P('sp', 'tp'), may hold values from -0.09375 to 0.09375
- key_weight: bfloat16 [4096, 3072], P('sp', 'tp'), may hold values from -0.09375 to 0.09375
- value_weight: bfloat16 [4096, 3072], P('sp', 'tp'), may hold values from -0.09375 to 0.09375
- merge_weight: bfloat16 [1024, 4096], P('tp', 'sp'), may hold values from -1.5 to 1.5
Outputs:
- attended: bfloat16 [2048, 4096], P(('sp', 'tp'))
All inputs are finite; a program needn't handle non-finite values.
Results may differ from a plain program's by a relative error of at most 0.013.
Values may be sent and summed in bfloat16 or wider, within the bound.
A program may use at most 128 MiB of HBM per device.

v0:
```python
import jax
import jax.numpy as jnp
from jax import lax
from jax.sharding import PartitionSpec as P

HEAD = 64
HEAD_GROUPS = 3
SPAN = 128
DILATION_MIDDLE = 4
DILATION_WIDEST = 8


rope_base = 500000.0


def passed_along(value, axis, steps):
    count = lax.axis_size(axis)
    leading, last = (max(0, -steps), min(count, count - steps))
    return lax.ppermute(value, axis, [(source, source + steps) for source in range(leading, last)])


def rotate(channels, angle_pos):
    half_width = channels.shape[-1] // 2
    frequency = rope_base ** (
        -jnp.arange(0, half_width, dtype=jnp.float32) * 2.0 / channels.shape[-1]
    )
    angles = angle_pos[:, None] * frequency[None, :]
    cosine = jnp.cos(angles)[:, None, None, :]
    sine_part = jnp.sin(angles)[:, None, None, :]
    first_half = channels[..., :half_width]
    second_half = channels[..., half_width:]
    return jnp.concatenate(
        [
            first_half * cosine - second_half * sine_part,
            second_half * cosine + first_half * sine_part,
        ],
        axis=-1,
    )


def window_mix(queries, kv_buffer, buffer_start, dilation):
    tok_rows = queries.shape[0]
    local_heads = queries.shape[1]
    query_steps = tok_rows // dilation
    class_rows = kv_buffer.shape[0] // dilation
    kept_rows = SPAN + query_steps
    classes = kv_buffer.reshape(class_rows, dilation, kv_buffer.shape[1])[class_rows - kept_rows :]
    key_rows = classes[:, :, : local_heads * HEAD].reshape(kept_rows, dilation, local_heads, HEAD)
    value_entries = classes[:, :, local_heads * HEAD :].reshape(
        kept_rows, dilation, local_heads, HEAD
    )
    query_cls = queries.reshape(query_steps, dilation, local_heads, HEAD)
    scores = jnp.einsum(
        "adhc,rdhc->dhar", query_cls, key_rows, preferred_element_type=jnp.float32
    ) * HEAD ** (-0.5)
    step_gap = (
        SPAN
        + jnp.arange(query_steps, dtype=jnp.int32)[:, None]
        - jnp.arange(kept_rows, dtype=jnp.int32)[None, :]
    )
    key_pos = (
        buffer_start
        + (class_rows - kept_rows + jnp.arange(kept_rows, dtype=jnp.int32))[None, :] * dilation
        + jnp.arange(dilation, dtype=jnp.int32)[:, None]
    )
    allowed = ((step_gap >= 0) & (step_gap <= SPAN))[None, :, :] & (key_pos >= 0)[:, None, :]
    scores = jnp.where(allowed[:, None], scores, -jnp.inf)
    row_max = jnp.max(scores, axis=-1, keepdims=True)
    expo = jnp.where(allowed[:, None], jnp.exp(scores - row_max), 0.0)
    denominator = jnp.sum(expo, axis=-1)
    rounded = expo.astype(jnp.bfloat16)
    mixed = jnp.einsum(
        "dhar,rdhc->adhc", rounded, value_entries, preferred_element_type=jnp.float32
    )
    mixed = mixed / jnp.transpose(denominator, (2, 0, 1))[..., None]
    mixed = mixed.reshape(tok_rows, local_heads, HEAD)
    log_total = jnp.transpose(row_max[..., 0] + jnp.log(denominator), (2, 0, 1)).reshape(
        tok_rows, local_heads
    )
    return (mixed, log_total)


def reach_doubling(kv_pairs, reach_counts, tok_rows):
    buffers = list(kv_pairs)
    stride = 1
    while stride <= max(reach_counts):
        members = [
            grp_index for grp_index in range(len(kv_pairs)) if reach_counts[grp_index] >= stride
        ]
        counts = [min(stride, reach_counts[grp_index] - stride + 1) for grp_index in members]
        outgoing = jnp.concatenate(
            [
                buffers[grp_index][buffers[grp_index].shape[0] - count_one * tok_rows :]
                for grp_index, count_one in zip(members, counts)
            ],
            axis=0,
        )
        incoming = passed_along(outgoing, "sp", stride)
        cursor = 0
        for grp_index, count_one in zip(members, counts):
            buffers[grp_index] = jnp.concatenate(
                [incoming[cursor : cursor + count_one * tok_rows], buffers[grp_index]], axis=0
            )
            cursor = cursor + count_one * tok_rows
        stride = stride * 2
    return buffers


def per_device(activity, query_weight, key_weight, value_weight, merge_weight):
    collected_rows = lax.all_gather(activity, "tp", axis=1, tiled=True)
    tok_rows = collected_rows.shape[0]
    col_width = query_weight.shape[1]
    local_heads = col_width // (HEAD_GROUPS * HEAD)
    offset = lax.axis_index("sp") * tok_rows
    pieces = (
        lax.all_gather(query_weight, "sp", axis=0, tiled=True),
        lax.all_gather(key_weight, "sp", axis=0, tiled=True),
        lax.all_gather(value_weight, "sp", axis=0, tiled=True),
    )
    query_sum, key_sum, value_sum = tuple(
        (
            jnp.dot(collected_rows, weight_piece, preferred_element_type=jnp.float32)
            for weight_piece in pieces
        )
    )
    query_pos = offset + jnp.arange(tok_rows, dtype=jnp.int32)
    angle_pos = query_pos.astype(jnp.float32)
    query_all = rotate(
        query_sum.reshape(tok_rows, local_heads, HEAD_GROUPS, HEAD), angle_pos
    ).astype(jnp.bfloat16)
    key_all = rotate(key_sum.reshape(tok_rows, local_heads, HEAD_GROUPS, HEAD), angle_pos).astype(
        jnp.bfloat16
    )
    value_all = value_sum.reshape(tok_rows, local_heads, HEAD_GROUPS, HEAD).astype(jnp.bfloat16)
    group_dilations = (1, DILATION_MIDDLE, DILATION_WIDEST)
    reach_counts = [-(-(SPAN * dilation) // tok_rows) for dilation in group_dilations]
    kv_pairs = [
        jnp.concatenate(
            [
                key_all[:, :, grp_index].reshape(tok_rows, local_heads * HEAD),
                value_all[:, :, grp_index].reshape(tok_rows, local_heads * HEAD),
            ],
            axis=1,
        )
        for grp_index in range(HEAD_GROUPS)
    ]
    buffers = reach_doubling(kv_pairs, reach_counts, tok_rows)
    mixed_list = []
    total_list = []
    for grp_index in range(HEAD_GROUPS):
        buffer_start = offset - reach_counts[grp_index] * tok_rows
        mixed, log_total = window_mix(
            query_all[:, :, grp_index], buffers[grp_index], buffer_start, group_dilations[grp_index]
        )
        mixed_list.append(mixed)
        total_list.append(log_total)
    total_stack = jnp.stack(total_list)
    peak_total = jnp.max(total_stack, axis=0)
    shifted = jnp.exp(total_stack - peak_total)
    group_weight = shifted / jnp.sum(shifted, axis=0)
    merged = jnp.sum(group_weight[..., None] * jnp.stack(mixed_list), axis=0)
    merged = merged.astype(jnp.bfloat16).reshape(tok_rows, local_heads * HEAD)
    merge_full = lax.all_gather(merge_weight, "sp", axis=1, tiled=True)
    return lax.psum_scatter(
        jnp.dot(merged, merge_full, preferred_element_type=jnp.float32).astype(jnp.bfloat16),
        "tp",
        scatter_dimension=0,
        tiled=True,
    )


def solution(mesh):
    placed = (P("sp", "tp"), P("sp", "tp"), P("sp", "tp"), P("sp", "tp"), P("tp", "sp"))
    return jax.shard_map(
        per_device, mesh=mesh, in_specs=placed, out_specs=P(("sp", "tp"), None), check_vma=False
    )
```

profile of v0, /device:TPU:25, one launch (start us, length us, event | category | flops | bytes accessed | tf_op | source)
XLA Modules:
  0.0 470.9 jit_solution(17329959254257123349)
XLA Ops:
  6.5 0.7 all-gather.6.cloned.1.call-update
  7.3 0.7 all-gather.8.cloned.1.call-update
  8.1 0.7 all-gather.10.cloned.1.call-update
  8.8 0.5 all-gather.12.cloned.1.call-update
  9.4 0.5 all-gather.14.cloned.1.call-update
  10.5 0.7 broadcast_and_fusion
  11.1 21.7 %all-gather.6.cloned.1.call-done = bf16[256,4096]{1,0:T(8,128)(2,1)} async-done(((bf16[256,1024]{1,0:T(8,128)(2,1)}), bf16[256,4096]{1,0:T(8,128)(2,1)}) %all-gather.6.cloned.1.call-update) | async-done | bytes 2097168 | tf_op jit(solution)/shard_map/all_gather | solution.py:110
  32.9 98.7 %all-gather.8.cloned.1.call-done = bf16[4096,768]{1,0:T(8,128)(2,1)} async-done(((bf16[512,768]{1,0:T(8,128)(2,1)}), bf16[4096,768]{1,0:T(8,128)(2,1)}) %all-gather.8.cloned.1.call-update) | async-done | bytes 6291472 | tf_op jit(solution)/shard_map/all_gather | solution.py:116
  131.5 6.0 %fusion.63 = f32[256,768]{0,1:T(8,128)S(1)} fusion(bf16[256,4096]{1,0:T(8,128)(2,1)} %all-gather.6.cloned.1.call-done, bf16[4096,768]{1,0:T(8,128)(2,1)} %all-gather.8.cloned.1.call-done), kind=kOutput, calls=%fused_computation.118 | convolution fusion | flops 1610612736 | bytes 9175040 | tf_op jit(solution)/shard_map/dot_general | solution.py:122
  137.6 93.0 %all-gather.10.cloned.1.call-done = bf16[4096,768]{1,0:T(8,128)(2,1)} async-done(((bf16[512,768]{1,0:T(8,128)(2,1)}), bf16[4096,768]{1,0:T(8,128)(2,1)}) %all-gather.10.cloned.1.call-update) | async-done | bytes 6291472 | tf_op jit(solution)/shard_map/all_gather | solution.py:117
  230.6 6.0 %fusion.64 = f32[256,768]{0,1:T(8,128)S(1)} fusion(bf16[256,4096]{1,0:T(8,128)(2,1)} %all-gather.6.cloned.1.call-done, bf16[4096,768]{1,0:T(8,128)(2,1)} %all-gather.10.cloned.1.call-done), kind=kOutput, calls=%fused_computation.119 | convolution fusion | flops 1610612736 | bytes 9175040 | tf_op jit(solution)/shard_map/dot_general | solution.py:122
  236.7 92.9 %all-gather.12.cloned.1.call-done = bf16[4096,768]{1,0:T(8,128)(2,1)} async-done(((bf16[512,768]{1,0:T(8,128)(2,1)}), bf16[4096,768]{1,0:T(8,128)(2,1)}) %all-gather.12.cloned.1.call-update) | async-done | bytes 6291472 | tf_op jit(solution)/shard_map/all_gather | solution.py:118
  329.6 5.2 %convolution_convert_fusion.1 = bf16[256,768]{1,0:T(8,128)(2,1)S(1)} fusion(bf16[256,4096]{1,0:T(8,128)(2,1)} %all-gather.6.cloned.1.call-done, bf16[4096,768]{1,0:T(8,128)(2,1)} %all-gather.12.cloned.1.call-done), kind=kOutput, calls=%fused_computation.10 | convolution fusion | flops 1610809344 | bytes 8781824 | tf_op jit(solution)/shard_map/dot_general | solution.py:122
  335.0 0.2 subtract_convert_fusion.1
  335.3 0.9 maximum_maximum_fusion.1
  336.3 2.2 collective-permute-start
  338.8 0.7 pad_maximum_fusion.3
  339.6 1.3 collective-permute-start.2
  341.0 25.7 %collective-permute-done = bf16[768,512]{0,1:T(8,128)(2,1)} collective-permute-done((bf16[768,512]{0,1:T(8,128)(2,1)}, bf16[768,512]{0,1:T(8,128)(2,1)}, u32[]{:S(2)}, u32[]{:S(2)}) %collective-permute-start) | collective-permute-done | bytes 786464 | tf_op jit(solution)/shard_map/ppermute | solution.py:19
  366.7 1.2 fusion.54
  368.1 1.5 collective-permute-start.1
  369.5 0.5 fusion.62
  370.1 0.6 fusion.3
  370.7 1.2 fusion.7
  371.9 0.6 fusion.47
  372.5 26.1 %collective-permute-done.1 = bf16[768,512]{0,1:T(8,128)(2,1)S(1)} collective-permute-done((bf16[768,512]{0,1:T(8,128)(2,1)S(1)}, bf16[768,512]{0,1:T(8,128)(2,1)S(1)}, u32[]{:S(2)}, u32[]{:S(2)}) %collective-permute-start.1) | collective-permute-done | bytes 786464 | tf_op jit(solution)/shard_map/ppermute | solution.py:19
  398.6 0.8 copy-done.3
  399.5 0.3 copy.83
  400.0 1.0 fusion.55
  401.0 0.3 copy.84
  401.3 0.4 fusion.61
  401.7 1.0 copy-done
  402.7 0.4 fusion.9
  403.2 0.7 stack_reshape.19
  403.9 0.7 stack.13
  404.8 0.7 copy.88
  405.6 0.6 copy.89
  406.4 0.4 fusion.60
  406.9 0.4 fusion.11
  407.6 1.1 copy.96
  408.7 2.3 fusion.5
  411.0 1.3 copy.97
  412.4 1.4 copy.98
  413.9 1.7 fusion.4
  415.6 0.3 copy.130
  416.3 0.2 copy-done.8
  416.7 3.7 convolution_convert_fusion
  420.3 43.8 %reduce-scatter.2.cloned.1.call-done = bf16[64,4096]{1,0:T(8,128)(2,1)} async-done(((bf16[256,4096]{1,0:T(8,128)(2,1)}), bf16[64,4096]{1,0:T(8,128)(2,1)}) %reduce-scatter.2.cloned.1.call-update) | async-done | bytes 524304 | tf_op jit(solution)/shard_map/reduce_scatter | solution.py:164
  (91 shorter events, 3.5 us)
Async XLA Ops:
  6.5 26.3 %all-gather.6.cloned.1.call-start = ((), (), s32[]{:S(2)}) async-start(), calls=%async_computation.1 | async-start | bytes 2621440 | tf_op jit(solution)/shard_map/all_gather | solution.py:110
  7.3 124.3 %all-gather.8.cloned.1.call-start = ((), (), s32[]{:S(2)}) async-start(), calls=%async_computation.2 | async-start | bytes 7077888 | tf_op jit(solution)/shard_map/all_gather | solution.py:116
  8.0 222.6 %all-gather.10.cloned.1.call-start = ((), (), s32[]{:S(2)}) async-start(), calls=%async_computation.3 | async-start | bytes 7077888 | tf_op jit(solution)/shard_map/all_gather | solution.py:117
  8.7 320.8 %all-gather.12.cloned.1.call-start = ((), (), s32[]{:S(2)}) async-start(), calls=%async_computation.4 | async-start | bytes 7077888 | tf_op jit(solution)/shard_map/all_gather | solution.py:118
  9.3 407.3 %all-gather.14.cloned.1.call-start = ((), (), s32[]{:S(2)}) async-start(), calls=%async_computation.5 | async-start | bytes 2359296 | tf_op jit(solution)/shard_map/all_gather | solution.py:163
  9.9 454.2 %reduce-scatter.2.cloned.1.call-start = ((), (), s32[]{:S(2)}) async-start(), calls=%async_computation.6 | async-start | bytes 2621440 | tf_op jit(solution)/shard_map/reduce_scatter | solution.py:164
  336.3 30.4 %collective-permute-start = (bf16[768,512]{0,1:T(8,128)(2,1)}, bf16[768,512]{0,1:T(8,128)(2,1)}, u32[]{:S(2)}, u32[]{:S(2)}) collective-permute-start(bf16[768,512]{0,1:T(8,128)(2,1)} %maximum_maximum_fusion.1), channel_id=1, source_target_pairs={{0,4},{4,8},{8,12},{12,16},{16,20},{20,24},{24,28},{1,5},{5,9},{9,... | collective-permute-start | bytes 2359304 | tf_op jit(solution)/shard_map/ppermute | solution.py:19
  338.5 63.2 %copy-start.6 = (pred[4,64,192]{2,1,0:T(8,128)(4,1)}, pred[4,64,192]{2,1,0:T(8,128)(4,1)S(1)}, u32[]{:S(2)}) copy-start(pred[4,64,192]{2,1,0:T(8,128)(4,1)S(1)} %broadcast_and_fusion.1) | copy-start | bytes 147460
  339.6 65.2 %collective-permute-start.2 = (bf16[256,512]{0,1:T(8,128)(2,1)}, bf16[256,512]{0,1:T(8,128)(2,1)S(1)}, u32[]{:S(2)}, u32[]{:S(2)}) collective-permute-start(bf16[256,512]{0,1:T(8,128)(2,1)} %pad_maximum_fusion.3), channel_id=1, source_target_pairs={{0,16},{4,20},{8,24},{12,28},{1,17},{5,21},{9,25},{13,29},{2,18},{... | collective-permute-start | bytes 786440 | tf_op jit(solution)/shard_map/ppermute | solution.py:19
  368.1 30.5 %collective-permute-start.1 = (bf16[768,512]{0,1:T(8,128)(2,1)S(1)}, bf16[768,512]{0,1:T(8,128)(2,1)S(1)}, u32[]{:S(2)}, u32[]{:S(2)}) collective-permute-start(bf16[768,512]{0,1:T(8,128)(2,1)S(1)} %maximum_maximum_fusion.2), channel_id=1, source_target_pairs={{0,8},{4,12},{8,16},{12,20},{16,24},{20,28},{1,9},{5,13},{9,17},{1... | collective-permute-start | bytes 2359304 | tf_op jit(solution)/shard_map/ppermute | solution.py:19
  370.1 1.8 copy-start.11
  370.7 27.9 %copy-start.13 = (f32[4,256]{1,0:T(4,128)}, f32[4,256]{1,0:T(4,128)S(1)}, u32[]{:S(2)}) copy-start(f32[4,256]{1,0:T(4,128)S(1)} %fusion.3) | copy-start | bytes 12292
  398.6 0.9 copy-start.3
  401.3 3.4 copy-start.4
  401.6 1.0 copy-start
  401.7 3.2 copy-start.9
  403.1 1.7 copy-start.17
  405.6 0.8 copy-start.5
  406.4 1.2 copy-start.2
  406.8 1.9 copy-start.1
  406.8 1.9 copy-start.7
  406.8 1.9 copy-start.10
  406.8 1.9 copy-start.18
  415.6 0.7 copy-start.12
  415.6 0.7 copy-start.14
  415.6 0.7 copy-start.19
  415.6 0.7 copy-start.15
  415.6 0.7 copy-start.16
  415.6 1.0 copy-start.8
Sparse Core Ops, SparseCore 0:
  8.9 23.9 all-gather.5
  35.0 96.4 all-gather.7
  133.7 96.8 all-gather.9
  232.7 96.8 all-gather.11
  331.5 60.9 all-gather.13
  420.5 43.5 reduce-scatter.1
where the time goes:
time: 473 us; the launch traced here: 471 us
  waiting for transfers between devices  405 us (86%)
  matrix products  27.2 us (6%)
  between operations  14.1 us (3%)
  local copies, waits for them, and re-layouts  13.8 us (3%)
  other arithmetic  5.64 us (1%)
  starting transfers between devices  5.1 us (1%)
    all_gather x1, waiting for transfers between devices, per_device(): lax.all_gather(query_weight, 'sp', axis=0, tiled=True)  98.7 us
    all_gather x1, waiting for transfers between devices, per_device(): lax.all_gather(key_weight, 'sp', axis=0, tiled=True)  93 us
    all_gather x1, waiting for transfers between devices, per_device(): lax.all_gather(value_weight, 'sp', axis=0, tiled=True)  92.9 us
    ppermute x3, waiting for transfers between devices, passed_along(): lax.ppermute(value, axis, [(source, source + steps) for source in range(l...  51.7 us
    reduce_scatter x1, waiting for transfers between devices, per_device(): lax.psum_scatter(jnp.dot(merged, merge_full, preferred_element_type=jnp.f...  43.8 us
    all_gather x1, waiting for transfers between devices, per_device(): collected_rows = lax.all_gather(activity, 'tp', axis=1, tiled=True)  21.7 us
    dot_general x3, matrix products, per_device(): jnp.dot(collected_rows, weight_piece, preferred_element_type=jnp.float32)  17.1 us
  transfers between devices with their start and end apart: 9, of which 7 were waited for; matrix products, arithmetic and copies ran while one was open for 9% of the time, Pallas kernels for 0%

commit v1 on v0

v1 whole, which is shorter than its diff:
```python
import functools

import jax
import jax.numpy as jnp
from jax import lax
from jax.experimental import pallas as pl
from jax.experimental.pallas import tpu as pltpu
from jax.sharding import PartitionSpec as P

HEAD = 64
HEAD_GROUPS = 3
SPAN = 128
DILATIONS = (1, 4, 8)
MESH = pl.DeviceIdType.MESH

rope_base = 500000.0


def project_kernel(
    G, R, act, wq, wk, wv, out,
    a_buf, w_buf, c_buf, r_buf,
    local_sem, swap_send, swap_recv, fan_send, fan_recv,
    w_send, w_recv, c_send, c_recv,
):
    s = lax.axis_index("sp")
    t = lax.axis_index("tp")
    g = lax.div(s, R)
    r = lax.rem(s, R)
    tok = act.shape[0]
    krows = wq.shape[0]
    width = wq.shape[1] // G
    pairs = G // 2
    weights = (wq, wk, wv)

    swap_dev = (t * R + r, g)
    barrier = pltpu.get_barrier_semaphore()

    def greet(dev):
        pl.semaphore_signal(barrier, inc=1, device_id=dev, device_id_type=MESH)

    for i in range(1, G):
        greet((s, lax.rem(t + i, G)))
        greet((lax.rem(g + i, G) * R + r, t))
    for i in range(1, R):
        greet((g * R + lax.rem(r + i, R), t))

    @pl.when(g != t)
    def _():
        greet(swap_dev)

    pl.semaphore_wait(barrier, 2 * (G - 1) + (R - 1) + jnp.where(g != t, 1, 0))

    def swap_copy():
        return pltpu.make_async_remote_copy(
            src_ref=act, dst_ref=a_buf.at[g], send_sem=swap_send, recv_sem=swap_recv,
            device_id=swap_dev, device_id_type=MESH)

    def swap_local():
        return pltpu.make_async_copy(act, a_buf.at[t], local_sem)

    @pl.when(g != t)
    def _():
        swap_copy().start()

    @pl.when(g == t)
    def _():
        swap_local().start()

    def pair_at(stage):
        return lax.rem(lax.div(g, 2) + 1 + stage, pairs)

    def pair_cols(stage):
        return pl.ds(pl.multiple_of(pair_at(stage) * (2 * width), 128), 2 * width)

    def w_copy(stage, i, x):
        cols = pair_cols(stage)
        return pltpu.make_async_remote_copy(
            src_ref=weights[x].at[:, cols], dst_ref=w_buf.at[i - 1, x, :, cols],
            send_sem=w_send.at[stage, i - 1, x], recv_sem=w_recv.at[stage, i - 1, x],
            device_id=(g * R + lax.rem(r + R - i, R), t), device_id_type=MESH)

    for stage in range(pairs):
        for i in range(1, R):
            for x in range(3):
                w_copy(stage, i, x).start()

    @pl.when(g != t)
    def _():
        swap_copy().wait_recv()

    @pl.when(g == t)
    def _():
        swap_local().wait()

    def fan_copy(i):
        return pltpu.make_async_remote_copy(
            src_ref=a_buf.at[t], dst_ref=a_buf.at[t], send_sem=fan_send.at[i - 1],
            recv_sem=fan_recv.at[i - 1],
            device_id=(s, lax.rem(t + i, G)), device_id_type=MESH)

    def fan_arrival(i):
        slot = lax.rem(t + G - i, G)
        return pltpu.make_async_remote_copy(
            src_ref=a_buf.at[slot], dst_ref=a_buf.at[slot], send_sem=fan_send.at[i - 1],
            recv_sem=fan_recv.at[i - 1],
            device_id=(s, lax.rem(t + i, G)), device_id_type=MESH)

    for i in range(1, G):
        fan_copy(i).start()
    for i in range(1, G):
        fan_arrival(i).wait_recv()

    def c_copy(stage, j, b):
        dest = pair_at(stage) * 2 + j
        rows = pl.ds(pl.multiple_of(b * tok, tok), tok)
        return pltpu.make_async_remote_copy(
            src_ref=c_buf.at[stage, j, rows], dst_ref=r_buf.at[g, rows],
            send_sem=c_send.at[stage, j, b], recv_sem=c_recv.at[g, b],
            device_id=(dest * R + r, t), device_id_type=MESH)

    for stage in range(pairs):
        for i in range(1, R):
            for x in range(3):
                w_copy(stage, i, x).wait_recv()
        cols = pair_cols(stage)

        @pl.loop(0, G)
        def _(b):
            parts = []
            for x in range(3):
                total = jnp.dot(
                    a_buf[b, :, pl.ds(pl.multiple_of(r * krows, 128), krows)],
                    weights[x][:, cols], preferred_element_type=jnp.float32)
                for i in range(1, R):
                    start = pl.multiple_of(lax.rem(r + i, R) * krows, 128)
                    total = total + jnp.dot(
                        a_buf[b, :, pl.ds(start, krows)], w_buf[i - 1, x, :, cols],
                        preferred_element_type=jnp.float32)
                parts.append(total)
            rows = pl.ds(pl.multiple_of(b * tok, tok), tok)
            for j in range(2):
                c_buf[stage, j, rows, :] = jnp.concatenate(
                    [part[:, j * width:(j + 1) * width] for part in parts], axis=1
                ).astype(jnp.bfloat16)
            for j in range(2):
                @pl.when(pair_at(stage) * 2 + j != g)
                def _():
                    c_copy(stage, j, b).start()

    def c_arrival(source, b):
        rows = pl.ds(pl.multiple_of(b * tok, tok), tok)
        return pltpu.make_async_remote_copy(
            src_ref=r_buf.at[source, rows], dst_ref=r_buf.at[source, rows],
            send_sem=c_send.at[0, 0, b], recv_sem=c_recv.at[source, b],
            device_id=(s, t), device_id_type=MESH)

    mine = lax.rem(g, 2)

    @pl.loop(0, G)
    def _(b):
        rows = pl.ds(pl.multiple_of(b * tok, tok), tok)
        total = c_buf[pairs - 1, mine, rows, :].astype(jnp.float32)
        for i in range(1, G):
            source = lax.rem(g + i, G)
            c_arrival(source, b).wait_recv()
            total = total + r_buf[source, rows, :].astype(jnp.float32)
        out[rows, :] = total

    @pl.when(g != t)
    def _():
        swap_copy().wait_send()

    for i in range(1, G):
        fan_copy(i).wait_send()
    for stage in range(pairs):
        for i in range(1, R):
            for x in range(3):
                w_copy(stage, i, x).wait_send()
        for j in range(2):
            @pl.when(pair_at(stage) * 2 + j != g)
            def _():
                @pl.loop(0, G)
                def _(b):
                    c_copy(stage, j, b).wait_send()


def project(activity, wq, wk, wv, G, R):
    tok, feat = activity.shape
    krows, col_width = wq.shape
    width = 3 * (col_width // G)
    pairs = G // 2
    rows = G * tok
    dma = pltpu.SemaphoreType.DMA
    return pl.pallas_call(
        functools.partial(project_kernel, G, R),
        out_shape=jax.ShapeDtypeStruct((rows, width), jnp.float32),
        in_specs=[pl.BlockSpec(memory_space=pltpu.VMEM)] * 4,
        out_specs=pl.BlockSpec(memory_space=pltpu.VMEM),
        scratch_shapes=[
            pltpu.VMEM((G, tok, feat), jnp.bfloat16),
            pltpu.VMEM((R - 1, 3, krows, col_width), jnp.bfloat16),
            pltpu.VMEM((pairs, 2, rows, width), jnp.bfloat16),
            pltpu.VMEM((G, rows, width), jnp.bfloat16),
            dma, dma, dma, dma((G - 1,)), dma((G - 1,)),
            dma((pairs, R - 1, 3)), dma((pairs, R - 1, 3)),
            dma((pairs, 2, G)), dma((G, G)),
        ],
        compiler_params=pltpu.CompilerParams(
            collective_id=0, has_side_effects=True, vmem_limit_bytes=58 * 2**20),
        cost_estimate=pl.CostEstimate(
            flops=2 * rows * feat * 3 * col_width, bytes_accessed=300 * 2**20, transcendentals=0),
    )(activity, wq, wk, wv)


def rotate(channels, angle_pos):
    half_width = channels.shape[-1] // 2
    frequency = rope_base ** (
        -jnp.arange(0, half_width, dtype=jnp.float32) * 2.0 / channels.shape[-1]
    )
    angles = angle_pos[:, :, None] * frequency
    cosine = jnp.cos(angles)[:, :, None, :]
    sine_part = jnp.sin(angles)[:, :, None, :]
    first_half = channels[..., :half_width]
    second_half = channels[..., half_width:]
    return jnp.concatenate(
        [
            first_half * cosine - second_half * sine_part,
            second_half * cosine + first_half * sine_part,
        ],
        axis=-1,
    )


def window_mix(queries, key_rows, value_rows, first_pos, dilation):
    blocks, tok, _ = queries.shape
    steps = tok // dilation
    kept = SPAN + steps
    q = queries.reshape(blocks, steps, dilation, HEAD)
    k = key_rows.reshape(blocks, kept, dilation, HEAD)
    v = value_rows.reshape(blocks, kept, dilation, HEAD)
    scores = jnp.einsum("zadc,zrdc->zdar", q, k, preferred_element_type=jnp.float32)
    scores = scores * HEAD ** (-0.5)
    step_gap = (
        SPAN
        + jnp.arange(steps, dtype=jnp.int32)[:, None]
        - jnp.arange(kept, dtype=jnp.int32)[None, :]
    )
    key_pos = (
        first_pos[:, None, None]
        + jnp.arange(kept, dtype=jnp.int32)[None, None, :] * dilation
        + jnp.arange(dilation, dtype=jnp.int32)[None, :, None]
    )
    allowed = ((step_gap >= 0) & (step_gap <= SPAN))[None, None] & (key_pos >= 0)[:, :, None, :]
    scores = jnp.where(allowed, scores, -jnp.inf)
    row_max = jnp.max(scores, axis=-1, keepdims=True)
    expo = jnp.where(allowed, jnp.exp(scores - row_max), 0.0)
    denominator = jnp.sum(expo, axis=-1)
    mixed = jnp.einsum(
        "zdar,zrdc->zadc", expo.astype(jnp.bfloat16), v, preferred_element_type=jnp.float32
    )
    mixed = mixed / jnp.transpose(denominator, (0, 2, 1))[..., None]
    log_total = jnp.transpose(row_max[..., 0] + jnp.log(denominator), (0, 2, 1))
    return mixed.reshape(blocks, tok, HEAD), log_total.reshape(blocks, tok)


def per_device(activity, query_weight, key_weight, value_weight, merge_weight):
    G = lax.axis_size("tp")
    R = lax.axis_size("sp") // G
    s = lax.axis_index("sp")
    r = s % R
    tok = activity.shape[0]
    total_tok = G * R * tok
    group_cols = HEAD_GROUPS * HEAD
    merge_full = lax.all_gather(merge_weight, "sp", axis=1, tiled=True)
    qkv = project(activity, query_weight, key_weight, value_weight, G, R)
    block_start = (jnp.arange(G, dtype=jnp.int32) * R + r) * tok
    pos = block_start[:, None] + jnp.arange(tok, dtype=jnp.int32)[None, :]
    qkv = qkv.reshape(G, tok, 3, HEAD_GROUPS, HEAD)
    turned = rotate(
        qkv[:, :, :2].reshape(G, tok, 2 * HEAD_GROUPS, HEAD), pos.astype(jnp.float32)
    ).astype(jnp.bfloat16)
    queries = turned[:, :, :HEAD_GROUPS]
    kv = jnp.concatenate(
        [
            turned[:, :, HEAD_GROUPS:].reshape(G, tok, group_cols),
            qkv[:, :, 2].astype(jnp.bfloat16).reshape(G, tok, group_cols),
        ],
        axis=-1,
    )
    held = [kv]
    for i in range(1, R):
        perm = [(a * R + b, a * R + (b - i) % R) for a in range(G) for b in range(R)]
        held.append(lax.ppermute(kv, "sp", perm))
    ordered = jnp.roll(jnp.stack(held), r, axis=0)
    kv_all = jnp.transpose(ordered, (1, 0, 2, 3)).reshape(total_tok, 2 * group_cols)
    most = SPAN * DILATIONS[-1]
    kv_all = jnp.pad(kv_all, ((most, 0), (0, 0)))
    windows = jnp.stack([
        lax.dynamic_slice_in_dim(kv_all, (a * R + r) * tok, most + tok, 0) for a in range(G)
    ])
    mixed_list = []
    total_list = []
    for index, dilation in enumerate(DILATIONS):
        reach = SPAN * dilation
        near = windows[:, most - reach:]
        keys = near[:, :, index * HEAD:(index + 1) * HEAD]
        values = near[:, :, group_cols + index * HEAD:group_cols + (index + 1) * HEAD]
        mixed, log_total = window_mix(
            queries[:, :, index], keys, values, block_start - reach, dilation)
        mixed_list.append(mixed)
        total_list.append(log_total)
    total_stack = jnp.stack(total_list)
    shifted = jnp.exp(total_stack - jnp.max(total_stack, axis=0))
    group_weight = shifted / jnp.sum(shifted, axis=0)
    merged = jnp.sum(group_weight[..., None] * jnp.stack(mixed_list), axis=0).astype(jnp.bfloat16)
    groups = [[a * R + b for a in range(G)] for b in range(R)]
    merged = lax.all_to_all(merged, "sp", 0, 0, axis_index_groups=groups)
    merged = jnp.transpose(merged, (1, 0, 2)).reshape(tok, G * HEAD)
    return lax.psum_scatter(
        jnp.dot(merged, merge_full, preferred_element_type=jnp.float32).astype(jnp.bfloat16),
        "tp",
        scatter_dimension=0,
        tiled=True,
    )


def solution(mesh):
    placed = (P("sp", "tp"), P("sp", "tp"), P("sp", "tp"), P("sp", "tp"), P("tp", "sp"))
    return jax.shard_map(
        per_device, mesh=mesh, in_specs=placed, out_specs=P(("sp", "tp"), None), check_vma=False
    )
```

time: 473 us -> 301 us (0.64)
  waiting for transfers between devices: 405 us -> 48.6 us
  Pallas kernels: 0 us -> 154 us
  local copies, waits for them, and re-layouts: 13.8 us -> 43.6 us
  matrix products: 27.2 us -> 14.9 us
  blocking collectives: 0 us -> 8.23 us
  other arithmetic: 5.64 us -> 13.3 us
    all_gather x4 -> x0, waiting for transfers between devices: 306 us -> none  [the longest x1 98.7 us: per_device(): lax.all_gather(query_weight, 'sp', axis=0, tiled=True)]
    pallas_call x0 -> x1, Pallas kernels: none -> 154 us  [project(): pl.pallas_call(functools.partial(project_kernel, G, R), out_shape=jax.Sha...]
    ppermute x3 -> x1, waiting for transfers between devices: 51.7 us -> 15.3 us  [per_device(): held.append(lax.ppermute(kv, 'sp', perm))]
    dot_general x9 -> x6, matrix products: 23.6 us -> 11.3 us  [the longest x3 5.69 us: window_mix(): jnp.einsum('zadc,zrdc->zdar', q, k, preferred_element_type=jnp.float32)]
    reduce_scatter x1, waiting for transfers between devices: 43.8 us -> 33.2 us  [per_device(): lax.psum_scatter(jnp.dot(merged, merge_full, preferred_element_type=jnp.f...]
    dynamic_slice x0 -> x5, local copies, waits for them, and re-layouts: none -> 10.4 us  [per_device(): lax.dynamic_slice_in_dim(kv_all, (a * R + r) * tok, most + tok, 0)]
    all_to_all x0 -> x1, blocking collectives: none -> 8.23 us  [per_device(): merged = lax.all_to_all(merged, 'sp', 0, 0, axis_index_groups=groups)]
    slice x15 -> x12, local copies, waits for them, and re-layouts: 6.34 us -> 13.8 us  [the longest x2 4.5 us: per_device(): keys = near[:, :, index * HEAD:(index + 1) * HEAD]]
  transfers between devices with their start and end apart: 9 -> 3, of which waited for: 7 -> 2; matrix products, arithmetic and copies ran while one was open for 9% -> 19% of each run, Pallas kernels for 0% -> 0%
where the time goes in v1:
time: 301 us; the launch traced here: 298 us
  Pallas kernels  154 us (51%)
  waiting for transfers between devices  48.6 us (16%)
  local copies, waits for them, and re-layouts  43.6 us (14%)
  matrix products  14.9 us (5%)
  between operations  13.7 us (5%)
  other arithmetic  13.3 us (4%)
  blocking collectives  8.23 us (3%)
    pallas_call x1, Pallas kernels, project(): pl.pallas_call(functools.partial(project_kernel, G, R), out_shape=jax.Sha...  154 us
    reduce_scatter x1, waiting for transfers between devices, per_device(): lax.psum_scatter(jnp.dot(merged, merge_full, preferred_element_type=jnp.f...  33.2 us
    ppermute x1, waiting for transfers between devices, per_device(): held.append(lax.ppermute(kv, 'sp', perm))  15.3 us
    dynamic_slice x5, local copies, waits for them, and re-layouts, per_device(): lax.dynamic_slice_in_dim(kv_all, (a * R + r) * tok, most + tok, 0)  10.4 us
    all_to_all x1, blocking collectives, per_device(): merged = lax.all_to_all(merged, 'sp', 0, 0, axis_index_groups=groups)  8.23 us
  transfers between devices with their start and end apart: 3, of which 2 were waited for; matrix products, arithmetic and copies ran while one was open for 19% of the time, Pallas kernels for 0%

profile of v1, /device:TPU:25, one launch (start us, length us, event | category | flops | bytes accessed | tf_op | source)
XLA Modules:
  0.0 297.7 jit_solution(4478549274682123887)
XLA Ops:
  6.5 154.0 %shard_map.55 = f32[1024,576]{1,0:T(8,128)} custom-call(bf16[256,1024]{1,0:T(8,128)(2,1)} %act.1, bf16[512,768]{1,0:T(8,128)(2,1)} %wq.1, bf16[512,768]{1,0:T(8,128)(2,1)} %wk.1, bf16[512,768]{1,0:T(8,128)(2,1)} %wv.1), custom_call_target="tpu_custom_call" | custom-call | flops 4831838208 | bytes 314572800 | tf_op jit(solution)/shard_map/pallas_call | solution.py:194
  160.6 2.1 copy.73
  162.7 2.2 reshape.366
  164.9 1.3 slice.92
  166.2 0.8 copy.76
  166.9 0.7 slice-done
  168.9 1.1 copy-done.2
  170.1 1.3 collective-permute-start
  171.6 0.8 copy.87
  172.5 0.7 fusion.69
  173.2 0.9 copy.82
  174.1 0.6 add_compare_fusion.1
  174.7 0.6 add_compare_fusion.2
  175.4 0.6 add_compare_fusion
  176.1 0.8 fusion.44
  176.9 15.3 %collective-permute-done = bf16[4,256,384]{1,2,0:T(8,128)(2,1)S(1)} collective-permute-done((bf16[4,256,384]{1,2,0:T(8,128)(2,1)S(1)}, bf16[4,256,384]{1,2,0:T(8,128)(2,1)S(1)}, u32[]{:S(2)}, u32[]{:S(2)}) %collective-permute-start) | collective-permute-done | bytes 786464 | tf_op jit(solution)/shard_map/ppermute | solution.py:293
  192.2 0.9 copy-done.8
  193.1 2.5 fusion.3
  195.6 1.0 copy.77
  196.6 4.4 %pad_dynamic-slice_fusion.7 = (bf16[1280,384]{1,0:T(8,128)(2,1)}, bf16[1280,384]{1,0:T(8,128)(2,1)}, bf16[1280,384]{1,0:T(8,128)(2,1)S(1)}, bf16[1280,384]{1,0:T(8,128)(2,1)}) fusion(s32[]{:T(128)S(6)} %select_n.57, bf16[2048,384]{1,0:T(8,128)(2,1)S(1)} %bitcast.80, s32[]{:T(128)S(6)} %select_n.58, s32[]{:T(128)S(6)} %select_n.59, s32[]{:T(128)S(6)} %select_n.60), kind=kLoop, calls=%fused_computation.8 | loop fusion | bytes 5505040 | tf_op jit(solution)/shard_map/dynamic_slice | solution.py:299
  201.0 1.5 copy.81
  202.5 0.6 copy.80
  203.2 1.6 copy.79
  204.8 2.3 copy.78
  207.0 2.2 pad_maximum_fusion.4
  209.2 2.3 copy.88
  211.6 2.4 fusion.79
  214.0 1.0 copy-done.6
  215.5 0.7 stack_reshape.16
  216.3 1.9 pad_maximum_fusion.6
  218.2 2.2 copy.83
  220.3 1.9 fusion.80
  223.3 0.6 bitcast_add_fusion.1
  223.9 0.8 copy.86
  224.7 0.7 stack_reshape.15
  225.5 2.3 copy.97
  227.9 2.2 fusion.12
  230.1 1.1 copy.127
  231.2 1.9 copy.101
  233.1 2.2 copy.94
  235.3 2.8 fusion.15
  238.1 2.1 copy.96
  240.2 1.9 copy.100
  242.1 1.4 fusion.81
  243.5 0.6 fusion.17
  245.8 8.2 %all_to_all.5 = bf16[4,256,64]{1,2,0:T(8,128)(2,1)S(1)} all-to-all(bf16[4,256,64]{1,2,0:T(8,128)(2,1)S(1)} %fusion.24), channel_id=1, replica_groups={{0,8,16,24},{4,12,20,28},{1,9,17,25},{5,13,21,29},{2,10,18,26},{6,14,22..., dimensions={0} | all-to-all | bytes 262144 | tf_op jit(solution)/shard_map/all_to_all | solution.py:317
  254.0 3.6 %convolution_convert_fusion = bf16[256,4096]{1,0:T(8,128)(2,1)} fusion(bf16[256,256]{0,1:T(8,128)(2,1)S(1)} %bitcast.90, bf16[256,4096]{1,0:T(8,128)(2,1)} %all-gather.2.cloned.1.call-done), kind=kOutput, calls=%fused_computation | convolution fusion | flops 537919488 | bytes 4325376 | tf_op jit(solution)/shard_map/dot_general | solution.py:320
  257.7 33.2 %reduce-scatter.2.cloned.1.call-done = bf16[64,4096]{1,0:T(8,128)(2,1)} async-done(((bf16[256,4096]{1,0:T(8,128)(2,1)}), bf16[64,4096]{1,0:T(8,128)(2,1)}) %reduce-scatter.2.cloned.1.call-update) | async-done | bytes 524304 | tf_op jit(solution)/shard_map/reduce_scatter | solution.py:319
  (67 shorter events, 5.1 us)
Async XLA Ops:
  6.5 247.5 %all-gather.2.cloned.1.call-start = ((), (), s32[]{:S(2)}) async-start(), calls=%async_computation.2 | async-start | bytes 2359296 | tf_op jit(solution)/shard_map/all_gather | solution.py:274
  166.1 1.6 slice-start
  168.9 2.7 copy-start.1
  168.9 1.1 copy-start.2
  170.1 22.1 %collective-permute-start = (bf16[4,256,384]{1,2,0:T(8,128)(2,1)S(1)}, bf16[4,256,384]{1,2,0:T(8,128)(2,1)S(1)}, u32[]{:S(2)}, u32[]{:S(2)}) collective-permute-start(bf16[4,256,384]{1,2,0:T(8,128)(2,1)S(1)} %get-tuple-element.17), channel_id=1, source_target_pairs={{0,4},{4,0},{8,12},{12,8},{16,20},{20,16},{24,28},{28,24},{1,5},{5... | collective-permute-start | bytes 2359304 | tf_op jit(solution)/shard_map/ppermute | solution.py:293
  171.5 119.4 %reduce-scatter.2.cloned.1.call-start = ((), (), s32[]{:S(2)}) async-start(), calls=%async_computation.3 | async-start | bytes 2621440 | tf_op jit(solution)/shard_map/reduce_scatter | solution.py:319
  192.2 0.9 copy-start.8
  209.2 2.3 copy-start.9
  209.2 2.4 copy-start.10
  214.0 1.0 copy-start.6
  216.3 4.1 %copy-start.13 = (pred[4,4,192]{2,1,0:T(4,128)(4,1)S(1)}, pred[4,4,192]{2,1,0:T(4,128)(4,1)}, u32[]{:S(2)}) copy-start(pred[4,4,192]{2,1,0:T(4,128)(4,1)} %add_compare_fusion.1) | copy-start | bytes 9220
  222.3 1.0 copy-start.7
  225.5 2.3 copy-start.11
  230.1 5.2 %copy-start.14 = (pred[4,4,192]{2,1,0:T(4,128)(4,1)S(1)}, pred[4,4,192]{2,1,0:T(4,128)(4,1)}, u32[]{:S(2)}) copy-start(pred[4,4,192]{2,1,0:T(4,128)(4,1)} %add_compare_fusion.1) | copy-start | bytes 9220
  238.1 4.0 %copy-start.3 = (pred[256,384]{1,0:T(8,128)(4,1)S(1)}, pred[256,384]{1,0:T(8,128)(4,1)}, u32[]{:S(2)}) copy-start(pred[256,384]{1,0:T(8,128)(4,1)} %fusion.44) | copy-start | bytes 294916
  238.1 4.0 %copy-start.12 = (pred[4,384]{1,0:T(4,128)(4,1)S(1)}, pred[4,384]{1,0:T(4,128)(4,1)}, u32[]{:S(2)}) copy-start(pred[4,384]{1,0:T(4,128)(4,1)} %add_compare_fusion.2) | copy-start | bytes 4612
  243.5 0.7 copy-start.15
  243.5 0.7 copy-start.16
  243.5 1.2 copy-start
  244.7 0.9 copy-start.4
  244.7 1.0 copy-start.5
Sparse Core Ops, SparseCore 0:
  171.6 51.6 all-gather.1
  257.8 33.0 reduce-scatter.1

commit v2 on v1

--- a/solution.py
+++ b/solution.py
@@ -17,10 +17,10 @@
 
 
 def project_kernel(
-    G, R, act, wq, wk, wv, out,
-    a_buf, w_buf, c_buf, r_buf,
+    G, R, act, wq, wk, wv, cos_ref, sin_ref, out,
+    a_buf, w_buf, c_buf, r_buf, q_buf, kv_buf, o_buf, m_buf,
     local_sem, swap_send, swap_recv, fan_send, fan_recv,
-    w_send, w_recv, c_send, c_recv,
+    w_send, w_recv, c_send, c_recv, kv_send, kv_recv, m_send, m_recv,
 ):
     s = lax.axis_index("sp")
     t = lax.axis_index("tp")
@@ -155,6 +155,25 @@
             device_id=(s, t), device_id_type=MESH)
 
     mine = lax.rem(g, 2)
+    most = SPAN * DILATIONS[-1]
+    kv_buf[0:most, :] = jnp.zeros((most, 2 * width), jnp.bfloat16)
+
+    def kv_rows(b, part):
+        return pl.ds(pl.multiple_of(most + (b * R + part) * tok, 128), tok)
+
+    def kv_copy(i, b):
+        rows = kv_rows(b, r)
+        return pltpu.make_async_remote_copy(
+            src_ref=kv_buf.at[rows], dst_ref=kv_buf.at[rows],
+            send_sem=kv_send.at[i - 1, b], recv_sem=kv_recv.at[i - 1, b],
+            device_id=(g * R + lax.rem(r + R - i, R), t), device_id_type=MESH)
+
+    def kv_arrival(i, b):
+        rows = kv_rows(b, lax.rem(r + i, R))
+        return pltpu.make_async_remote_copy(
+            src_ref=kv_buf.at[rows], dst_ref=kv_buf.at[rows],
+            send_sem=kv_send.at[i - 1, b], recv_sem=kv_recv.at[i - 1, b],
+            device_id=(g * R + lax.rem(r + R - i, R), t), device_id_type=MESH)
 
     @pl.loop(0, G)
     def _(b):
@@ -164,7 +183,93 @@
             source = lax.rem(g + i, G)
             c_arrival(source, b).wait_recv()
             total = total + r_buf[source, rows, :].astype(jnp.float32)
-        out[rows, :] = total
+        turn = total[:, :2 * width]
+        half = HEAD // 2
+        ahead = jnp.concatenate([turn[:, half:], turn[:, :half]], axis=1)
+        behind = jnp.concatenate([turn[:, -half:], turn[:, :-half]], axis=1)
+        lane = lax.broadcasted_iota(jnp.int32, turn.shape, 1)
+        other = jnp.where((lane & (HEAD - 1)) < half, ahead, behind)
+        reps = 2 * width // cos_ref.shape[1]
+        cosine = jnp.concatenate([cos_ref[rows, :]] * reps, axis=1)
+        sine = jnp.concatenate([sin_ref[rows, :]] * reps, axis=1)
+        turned = turn * cosine + other * sine
+        q_buf[rows, :] = turned[:, :width].astype(jnp.bfloat16)
+        kv_buf[kv_rows(b, r), :] = jnp.concatenate(
+            [turned[:, width:], total[:, 2 * width:]], axis=1).astype(jnp.bfloat16)
+        for i in range(1, R):
+            kv_copy(i, b).start()
+
+    @pl.loop(0, G)
+    def _(b):
+        for i in range(1, R):
+            kv_arrival(i, b).wait_recv()
+
+    def m_copy(b):
+        return pltpu.make_async_remote_copy(
+            src_ref=o_buf.at[b], dst_ref=m_buf.at[g],
+            send_sem=m_send.at[b], recv_sem=m_recv.at[g],
+            device_id=(b * R + r, t), device_id_type=MESH)
+
+    def m_arrival(source):
+        return pltpu.make_async_remote_copy(
+            src_ref=m_buf.at[source], dst_ref=m_buf.at[source],
+            send_sem=m_send.at[source], recv_sem=m_recv.at[source],
+            device_id=(source * R + r, t), device_id_type=MESH)
+
+    @pl.loop(0, G)
+    def _(b):
+        rows = pl.ds(pl.multiple_of(b * tok, tok), tok)
+        first = (b * R + r) * tok
+        mixed_list = []
+        total_list = []
+        for index, dilation in enumerate(DILATIONS):
+            reach = SPAN * dilation
+            keys = reach + tok
+            near = pl.ds(pl.multiple_of(most - reach + first, 128), keys)
+            q = q_buf[rows, index * HEAD:(index + 1) * HEAD]
+            k = kv_buf[near, index * HEAD:(index + 1) * HEAD]
+            v = kv_buf[near, width + index * HEAD:width + (index + 1) * HEAD]
+            scores = lax.dot_general(
+                q, k, (((1,), (1,)), ((), ())), preferred_element_type=jnp.float32
+            ) * HEAD ** (-0.5)
+            col = lax.broadcasted_iota(jnp.int32, (tok, keys), 1)
+            gap = reach + lax.broadcasted_iota(jnp.int32, (tok, keys), 0) - col
+            allowed = (gap >= 0) & (gap <= reach) & (col >= reach - first)
+            if dilation > 1:
+                allowed = allowed & ((gap & (dilation - 1)) == 0)
+            scores = jnp.where(allowed, scores, -jnp.inf)
+            row_max = jnp.max(scores, axis=1, keepdims=True)
+            expo = jnp.exp(scores - row_max)
+            denominator = jnp.sum(expo, axis=1, keepdims=True)
+            mixed = jnp.dot(expo.astype(jnp.bfloat16), v, preferred_element_type=jnp.float32)
+            mixed_list.append(mixed / denominator)
+            total_list.append(row_max + jnp.log(denominator))
+        peak = jnp.maximum(jnp.maximum(total_list[0], total_list[1]), total_list[2])
+        shifted = [jnp.exp(one - peak) for one in total_list]
+        whole = shifted[0] + shifted[1] + shifted[2]
+        merged = sum(a / whole * b_ for a, b_ in zip(shifted, mixed_list)).astype(jnp.bfloat16)
+
+        @pl.when(b != g)
+        def _():
+            o_buf[b] = merged
+            m_copy(b).start()
+
+        @pl.when(b == g)
+        def _():
+            m_buf[b] = merged
+
+    for i in range(1, G):
+        m_arrival(lax.rem(g + i, G)).wait_recv()
+    out[...] = jnp.concatenate(
+        [m_buf[h].astype(jnp.float32) for h in range(G)], axis=1).astype(jnp.bfloat16)
+
+    for i in range(1, G):
+        m_copy(lax.rem(g + i, G)).wait_send()
+
+    @pl.loop(0, G)
+    def _(b):
+        for i in range(1, R):
+            kv_copy(i, b).wait_send()
 
     @pl.when(g != t)
     def _():
@@ -184,7 +289,7 @@
                     c_copy(stage, j, b).wait_send()
 
 
-def project(activity, wq, wk, wv, G, R):
+def project(activity, wq, wk, wv, cosine, sine, G, R):
     tok, feat = activity.shape
     krows, col_width = wq.shape
     width = 3 * (col_width // G)
@@ -193,135 +298,127 @@
     dma = pltpu.SemaphoreType.DMA
     return pl.pallas_call(
         functools.partial(project_kernel, G, R),
-        out_shape=jax.ShapeDtypeStruct((rows, width), jnp.float32),
-        in_specs=[pl.BlockSpec(memory_space=pltpu.VMEM)] * 4,
+        out_shape=jax.ShapeDtypeStruct((tok, G * HEAD), jnp.bfloat16),
+        in_specs=[pl.BlockSpec(memory_space=pltpu.VMEM)] * 6,
         out_specs=pl.BlockSpec(memory_space=pltpu.VMEM),
         scratch_shapes=[
             pltpu.VMEM((G, tok, feat), jnp.bfloat16),
             pltpu.VMEM((R - 1, 3, krows, col_width), jnp.bfloat16),
             pltpu.VMEM((pairs, 2, rows, width), jnp.bfloat16),
             pltpu.VMEM((G, rows, width), jnp.bfloat16),
+            pltpu.VMEM((rows, width // 3), jnp.bfloat16),
+            pltpu.VMEM((SPAN * DILATIONS[-1] + R * rows, 2 * (width // 3)), jnp.bfloat16),
+            pltpu.VMEM((G, tok, HEAD), jnp.bfloat16),
+            pltpu.VMEM((G, tok, HEAD), jnp.bfloat16),
             dma, dma, dma, dma((G - 1,)), dma((G - 1,)),
             dma((pairs, R - 1, 3)), dma((pairs, R - 1, 3)),
             dma((pairs, 2, G)), dma((G, G)),
+            dma((R - 1, G)), dma((R - 1, G)), dma((G,)), dma((G,)),
         ],
         compiler_params=pltpu.CompilerParams(
             collective_id=0, has_side_effects=True, vmem_limit_bytes=58 * 2**20),
         cost_estimate=pl.CostEstimate(
             flops=2 * rows * feat * 3 * col_width, bytes_accessed=300 * 2**20, transcendentals=0),
-    )(activity, wq, wk, wv)
-
-
-def rotate(channels, angle_pos):
-    half_width = channels.shape[-1] // 2
-    frequency = rope_base ** (
-        -jnp.arange(0, half_width, dtype=jnp.float32) * 2.0 / channels.shape[-1]
-    )
-    angles = angle_pos[:, :, None] * frequency
-    cosine = jnp.cos(angles)[:, :, None, :]
-    sine_part = jnp.sin(angles)[:, :, None, :]
-    first_half = channels[..., :half_width]
-    second_half = channels[..., half_width:]
-    return jnp.concatenate(
-        [
-            first_half * cosine - second_half * sine_part,
-            second_half * cosine + first_half * sine_part,
+    )(activity, wq, wk, wv, cosine, sine)
+
+
+def finish_kernel(merged, weight, out, near_out, near_in, far_out, far_in, held,
+                  near_send, near_recv, far_send, far_recv):
+    s = lax.axis_index("sp")
+    t = lax.axis_index("tp")
+    chunks = near_out.shape[0]
+    rows = out.shape[0]
+    cols = weight.shape[1] // chunks
+    low = lax.rem(t, 2)
+    near = t + 1 - 2 * low
+    far = lax.rem(t + 2, 4)
+    across = lax.rem(near + 2, 4)
+
+    barrier = pltpu.get_barrier_semaphore()
+    for peer in (near, far):
+        pl.semaphore_signal(barrier, inc=1, device_id=(s, peer), device_id_type=MESH)
+    pl.semaphore_wait(barrier, 2)
+
+    def near_copy(c):
+        return pltpu.make_async_remote_copy(
+            src_ref=near_out.at[c], dst_ref=near_in.at[c], send_sem=near_send.at[c],
+            recv_sem=near_recv.at[c], device_id=(s, near), device_id_type=MESH)
+
+    def far_copy(c):
+        return pltpu.make_async_remote_copy(
+            src_ref=far_out.at[c], dst_ref=far_in.at[c], send_sem=far_send.at[c],
+            recv_sem=far_recv.at[c], device_id=(s, far), device_id_type=MESH)
+
+    def part(owner, at):
+        picked = merged[pl.ds(pl.multiple_of(owner * rows, rows), rows), :]
+        return jnp.dot(picked, weight[:, at], preferred_element_type=jnp.float32)
+
+    @pl.loop(0, chunks)
+    def _(c):
+        at = pl.ds(pl.multiple_of(c * cols, 128), cols)
+        near_out[c, 0] = part(across, at).astype(jnp.bfloat16)
+        near_out[c, 1] = part(near, at).astype(jnp.bfloat16)
+        near_copy(c).start()
+        held[c, 0] = part(far, at)
+        held[c, 1] = part(t, at)
+
+    @pl.loop(0, chunks)
+    def _(c):
+        near_copy(c).wait_recv()
+        far_out[c] = (held[c, 0] + near_in[c, 0].astype(jnp.float32)).astype(jnp.bfloat16)
+        far_copy(c).start()
+        held[c, 1] = held[c, 1] + near_in[c, 1].astype(jnp.float32)
+
+    @pl.loop(0, chunks)
+    def _(c):
+        at = pl.ds(pl.multiple_of(c * cols, 128), cols)
+        far_copy(c).wait_recv()
+        out[:, at] = (held[c, 1] + far_in[c].astype(jnp.float32)).astype(jnp.bfloat16)
+
+    @pl.loop(0, chunks)
+    def _(c):
+        near_copy(c).wait_send()
+        far_copy(c).wait_send()
+
+
+def finish(merged, weight, chunks):
+    rows = merged.shape[0] // 4
+    cols = weight.shape[1] // chunks
+    dma = pltpu.SemaphoreType.DMA
+    return pl.pallas_call(
+        finish_kernel,
+        out_shape=jax.ShapeDtypeStruct((rows, weight.shape[1]), jnp.bfloat16),
+        in_specs=[pl.BlockSpec(memory_space=pltpu.VMEM)] * 2,
+        out_specs=pl.BlockSpec(memory_space=pltpu.VMEM),
+        scratch_shapes=[
+            pltpu.VMEM((chunks, 2, rows, cols), jnp.bfloat16),
+            pltpu.VMEM((chunks, 2, rows, cols), jnp.bfloat16),
+            pltpu.VMEM((chunks, rows, cols), jnp.bfloat16),
+            pltpu.VMEM((chunks, rows, cols), jnp.bfloat16),
+            pltpu.VMEM((chunks, 2, rows, cols), jnp.float32),
+            dma((chunks,)), dma((chunks,)), dma((chunks,)), dma((chunks,)),
         ],
-        axis=-1,
-    )
-
-
-def window_mix(queries, key_rows, value_rows, first_pos, dilation):
-    blocks, tok, _ = queries.shape
-    steps = tok // dilation
-    kept = SPAN + steps
-    q = queries.reshape(blocks, steps, dilation, HEAD)
-    k = key_rows.reshape(blocks, kept, dilation, HEAD)
-    v = value_rows.reshape(blocks, kept, dilation, HEAD)
-    scores = jnp.einsum("zadc,zrdc->zdar", q, k, preferred_element_type=jnp.float32)
-    scores = scores * HEAD ** (-0.5)
-    step_gap = (
-        SPAN
-        + jnp.arange(steps, dtype=jnp.int32)[:, None]
-        - jnp.arange(kept, dtype=jnp.int32)[None, :]
-    )
-    key_pos = (
-        first_pos[:, None, None]
-        + jnp.arange(kept, dtype=jnp.int32)[None, None, :] * dilation
-        + jnp.arange(dilation, dtype=jnp.int32)[None, :, None]
-    )
-    allowed = ((step_gap >= 0) & (step_gap <= SPAN))[None, None] & (key_pos >= 0)[:, :, None, :]
-    scores = jnp.where(allowed, scores, -jnp.inf)
-    row_max = jnp.max(scores, axis=-1, keepdims=True)
-    expo = jnp.where(allowed, jnp.exp(scores - row_max), 0.0)
-    denominator = jnp.sum(expo, axis=-1)
-    mixed = jnp.einsum(
-        "zdar,zrdc->zadc", expo.astype(jnp.bfloat16), v, preferred_element_type=jnp.float32
-    )
-    mixed = mixed / jnp.transpose(denominator, (0, 2, 1))[..., None]
-    log_total = jnp.transpose(row_max[..., 0] + jnp.log(denominator), (0, 2, 1))
-    return mixed.reshape(blocks, tok, HEAD), log_total.reshape(blocks, tok)
+        compiler_params=pltpu.CompilerParams(
+            collective_id=1, has_side_effects=True, vmem_limit_bytes=40 * 2**20),
+    )(merged, weight)
 
 
 def per_device(activity, query_weight, key_weight, value_weight, merge_weight):
     G = lax.axis_size("tp")
     R = lax.axis_size("sp") // G
-    s = lax.axis_index("sp")
-    r = s % R
+    r = lax.axis_index("sp") % R
     tok = activity.shape[0]
-    total_tok = G * R * tok
-    group_cols = HEAD_GROUPS * HEAD
     merge_full = lax.all_gather(merge_weight, "sp", axis=1, tiled=True)
-    qkv = project(activity, query_weight, key_weight, value_weight, G, R)
     block_start = (jnp.arange(G, dtype=jnp.int32) * R + r) * tok
-    pos = block_start[:, None] + jnp.arange(tok, dtype=jnp.int32)[None, :]
-    qkv = qkv.reshape(G, tok, 3, HEAD_GROUPS, HEAD)
-    turned = rotate(
-        qkv[:, :, :2].reshape(G, tok, 2 * HEAD_GROUPS, HEAD), pos.astype(jnp.float32)
-    ).astype(jnp.bfloat16)
-    queries = turned[:, :, :HEAD_GROUPS]
-    kv = jnp.concatenate(
-        [
-            turned[:, :, HEAD_GROUPS:].reshape(G, tok, group_cols),
-            qkv[:, :, 2].astype(jnp.bfloat16).reshape(G, tok, group_cols),
-        ],
-        axis=-1,
-    )
-    held = [kv]
-    for i in range(1, R):
-        perm = [(a * R + b, a * R + (b - i) % R) for a in range(G) for b in range(R)]
-        held.append(lax.ppermute(kv, "sp", perm))
-    ordered = jnp.roll(jnp.stack(held), r, axis=0)
-    kv_all = jnp.transpose(ordered, (1, 0, 2, 3)).reshape(total_tok, 2 * group_cols)
-    most = SPAN * DILATIONS[-1]
-    kv_all = jnp.pad(kv_all, ((most, 0), (0, 0)))
-    windows = jnp.stack([
-        lax.dynamic_slice_in_dim(kv_all, (a * R + r) * tok, most + tok, 0) for a in range(G)
-    ])
-    mixed_list = []
-    total_list = []
-    for index, dilation in enumerate(DILATIONS):
-        reach = SPAN * dilation
-        near = windows[:, most - reach:]
-        keys = near[:, :, index * HEAD:(index + 1) * HEAD]
-        values = near[:, :, group_cols + index * HEAD:group_cols + (index + 1) * HEAD]
-        mixed, log_total = window_mix(
-            queries[:, :, index], keys, values, block_start - reach, dilation)
-        mixed_list.append(mixed)
-        total_list.append(log_total)
-    total_stack = jnp.stack(total_list)
-    shifted = jnp.exp(total_stack - jnp.max(total_stack, axis=0))
-    group_weight = shifted / jnp.sum(shifted, axis=0)
-    merged = jnp.sum(group_weight[..., None] * jnp.stack(mixed_list), axis=0).astype(jnp.bfloat16)
-    groups = [[a * R + b for a in range(G)] for b in range(R)]
-    merged = lax.all_to_all(merged, "sp", 0, 0, axis_index_groups=groups)
-    merged = jnp.transpose(merged, (1, 0, 2)).reshape(tok, G * HEAD)
-    return lax.psum_scatter(
-        jnp.dot(merged, merge_full, preferred_element_type=jnp.float32).astype(jnp.bfloat16),
-        "tp",
-        scatter_dimension=0,
-        tiled=True,
-    )
+    pos = (block_start[:, None] + jnp.arange(tok, dtype=jnp.int32)[None, :]).reshape(G * tok)
+    half = HEAD // 2
+    frequency = rope_base ** (-jnp.arange(0, half, dtype=jnp.float32) * 2.0 / HEAD)
+    angles = pos.astype(jnp.float32)[:, None] * frequency[None, :]
+    cosine = jnp.tile(jnp.cos(angles), (1, 4))
+    sine = jnp.sin(angles)
+    sine = jnp.tile(jnp.concatenate([-sine, sine], axis=1), (1, 2))
+    merged = project(activity, query_weight, key_weight, value_weight, cosine, sine, G, R)
+    return finish(merged, merge_full, 8)
 
 
 def solution(mesh):

time: 301 us -> 227 us (0.75); the launches traced: 298 us -> 227 us
  Pallas kernels: 154 us -> 207 us
  waiting for transfers between devices: 48.6 us -> 0.73 us
  local copies, waits for them, and re-layouts: 43.6 us -> 5.36 us
  matrix products: 14.9 us -> 0 us
  other arithmetic: 13.3 us -> 0.65 us
  blocking collectives: 8.23 us -> 0 us
    reduce_scatter x1 -> x0, waiting for transfers between devices: 33.2 us -> none  [per_device(): lax.psum_scatter(jnp.dot(merged, merge_full, preferred_element_type=jnp.f...]
    pallas_call x1, Pallas kernels: 154 us -> 187 us  [project(): pl.pallas_call(functools.partial(project_kernel, G, R), out_shape=jax.Sha...]
    pallas_call x0 -> x1, Pallas kernels: none -> 19.6 us  [finish(): pl.pallas_call(finish_kernel, out_shape=jax.ShapeDtypeStruct((rows, weigh...]
    ppermute x1 -> x0, waiting for transfers between devices: 15.3 us -> none  [per_device(): held.append(lax.ppermute(kv, 'sp', perm))]
    dot_general x7 -> x0, matrix products: 14.9 us -> none  [the longest x3 5.69 us: window_mix(): jnp.einsum('zadc,zrdc->zdar', q, k, preferred_element_type=jnp.float32)]
    slice x12 -> x0, local copies, waits for them, and re-layouts: 13.8 us -> none  [the longest x2 4.5 us: per_device(): keys = near[:, :, index * HEAD:(index + 1) * HEAD]]
    dynamic_slice x5 -> x0, local copies, waits for them, and re-layouts: 10.4 us -> none  [per_device(): lax.dynamic_slice_in_dim(kv_all, (a * R + r) * tok, most + tok, 0)]
    all_to_all x1 -> x0, blocking collectives: 8.23 us -> none  [per_device(): merged = lax.all_to_all(merged, 'sp', 0, 0, axis_index_groups=groups)]
  transfers between devices with their start and end apart: 3 -> 1, of which waited for: 2 -> 0; matrix products, arithmetic and copies ran while one was open for 19% -> 1% of each run, Pallas kernels for 0% -> 82%
where the time goes in v2:
time: 227 us
  Pallas kernels  207 us (91%)
  between operations  13.5 us (6%)
  local copies, waits for them, and re-layouts  5.36 us (2%)
    pallas_call x1, Pallas kernels, project(): pl.pallas_call(functools.partial(project_kernel, G, R), out_shape=jax.Sha...  187 us
    pallas_call x1, Pallas kernels, finish(): pl.pallas_call(finish_kernel, out_shape=jax.ShapeDtypeStruct((rows, weigh...  19.6 us
  transfers between devices with their start and end apart: 1, of which 0 were waited for; matrix products, arithmetic and copies ran while one was open for 1% of the time, Pallas kernels for 82%

profile of v2, /device:TPU:25, one launch (start us, length us, event | category | flops | bytes accessed | tf_op | source)
XLA Modules:
  0.0 226.9 jit_solution(10681837947093851363)
XLA Ops:
  6.5 0.0 all-gather.2.cloned.1.call-start
  6.5 0.7 all-gather.2.cloned.1.call-update
  7.3 0.1 convert_bitcast_fusion
  7.4 0.5 fusion
  8.0 1.0 copy.7.sin_ref
  9.0 1.0 copy.6.cos_ref
  10.0 187.0 %shard_map.55.merged = bf16[256,256]{1,0:T(8,128)(2,1)} custom-call(bf16[256,1024]{1,0:T(8,128)(2,1)} %act.1, bf16[512,768]{1,0:T(8,128)(2,1)} %wq.1, bf16[512,768]{1,0:T(8,128)(2,1)} %wk.1, bf16[512,768]{1,0:T(8,128)(2,1)} %wv.1, f32[1024,128]{1,0:T(8,128)} %copy.6.cos_ref, f32[1024,128]{1,0:T(8,128)} %copy.7.sin_ref), custom_call_target="tpu_custom_call" | custom-call | flops 4831838208 | bytes 314572800 | tf_op jit(solution)/shard_map/pallas_call | solution.py:299
  197.1 0.0 all-gather.2.cloned.1.call-done.weight
  197.1 0.0 copy-start
  197.1 1.6 copy-done
  198.7 0.0 copy-start.1
  198.7 0.9 copy-done.1
  199.6 19.6 %shard_map.56 = bf16[64,4096]{1,0:T(8,128)(2,1)S(1)} custom-call(bf16[256,256]{1,0:T(8,128)(2,1)S(1)} %copy-done.1, bf16[256,4096]{1,0:T(8,128)(2,1)S(1)} %copy-done), custom_call_target="tpu_custom_call" | custom-call | tf_op jit(solution)/shard_map/pallas_call | solution.py:388
  219.2 0.8 copy.10
  (6 shorter events, 0.1 us)
Async XLA Ops:
  6.5 190.6 %all-gather.2.cloned.1.call-start = ((), (), s32[]{:S(2)}) async-start(), calls=%async_computation | async-start | bytes 2359296 | tf_op jit(solution)/shard_map/all_gather | solution.py:411
  197.1 1.6 copy-start
  198.7 0.9 copy-start.1
Sparse Core Ops, SparseCore 0:
  9.4 119.3 all-gather.1

commit v3 on v2

--- a/solution.py
+++ b/solution.py
@@ -175,8 +175,7 @@
             send_sem=kv_send.at[i - 1, b], recv_sem=kv_recv.at[i - 1, b],
             device_id=(g * R + lax.rem(r + R - i, R), t), device_id_type=MESH)
 
-    @pl.loop(0, G)
-    def _(b):
+    def gather_block(b):
         rows = pl.ds(pl.multiple_of(b * tok, tok), tok)
         total = c_buf[pairs - 1, mine, rows, :].astype(jnp.float32)
         for i in range(1, G):
@@ -199,11 +198,6 @@
         for i in range(1, R):
             kv_copy(i, b).start()
 
-    @pl.loop(0, G)
-    def _(b):
-        for i in range(1, R):
-            kv_arrival(i, b).wait_recv()
-
     def m_copy(b):
         return pltpu.make_async_remote_copy(
             src_ref=o_buf.at[b], dst_ref=m_buf.at[g],
@@ -216,8 +210,9 @@
             send_sem=m_send.at[source], recv_sem=m_recv.at[source],
             device_id=(source * R + r, t), device_id_type=MESH)
 
-    @pl.loop(0, G)
-    def _(b):
+    def attend(b):
+        for i in range(1, R):
+            kv_arrival(i, b).wait_recv()
         rows = pl.ds(pl.multiple_of(b * tok, tok), tok)
         first = (b * R + r) * tok
         mixed_list = []
@@ -257,6 +252,15 @@
         @pl.when(b == g)
         def _():
             m_buf[b] = merged
+
+    gather_block(0)
+
+    @pl.loop(1, G)
+    def _(b):
+        gather_block(b)
+        attend(b - 1)
+
+    attend(G - 1)
 
     for i in range(1, G):
         m_arrival(lax.rem(g + i, G)).wait_recv()

time: 227 us -> 225 us (level)
  Pallas kernels: 207 us -> 204 us
    pallas_call x1, Pallas kernels: 187 us -> 185 us  [project(): pl.pallas_call(functools.partial(project_kernel, G, R), out_shape=jax.Sha...]
where the time goes in v3:
time: 225 us
  Pallas kernels  204 us (91%)
  between operations  13.5 us (6%)
  local copies, waits for them, and re-layouts  5.36 us (2%)
    pallas_call x1, Pallas kernels, project(): pl.pallas_call(functools.partial(project_kernel, G, R), out_shape=jax.Sha...  185 us
    pallas_call x1, Pallas kernels, finish(): pl.pallas_call(finish_kernel, out_shape=jax.ShapeDtypeStruct((rows, weigh...  19.8 us
  transfers between devices with their start and end apart: 1, of which 0 were waited for; matrix products, arithmetic and copies ran while one was open for 1% of the time, Pallas kernels for 82%

profile of v3, /device:TPU:25, one launch (start us, length us, event | category | flops | bytes accessed | tf_op | source)
XLA Modules:
  0.0 224.5 jit_solution(12454757120080427047)
XLA Ops:
  6.5 0.0 all-gather.2.cloned.1.call-start
  6.5 0.7 all-gather.2.cloned.1.call-update
  7.3 0.1 convert_bitcast_fusion
  7.4 0.5 fusion
  8.0 1.0 copy.7.sin_ref
  9.0 1.0 copy.6.cos_ref
  10.0 184.5 %shard_map.55.merged = bf16[256,256]{1,0:T(8,128)(2,1)} custom-call(bf16[256,1024]{1,0:T(8,128)(2,1)} %act.1, bf16[512,768]{1,0:T(8,128)(2,1)} %wq.1, bf16[512,768]{1,0:T(8,128)(2,1)} %wk.1, bf16[512,768]{1,0:T(8,128)(2,1)} %wv.1, f32[1024,128]{1,0:T(8,128)} %copy.6.cos_ref, f32[1024,128]{1,0:T(8,128)} %copy.7.sin_ref), custom_call_target="tpu_custom_call" | custom-call | flops 4831838208 | bytes 314572800 | tf_op jit(solution)/shard_map/pallas_call | solution.py:303
  194.6 0.0 all-gather.2.cloned.1.call-done.weight
  194.6 0.0 copy-start
  194.6 1.6 copy-done
  196.2 0.0 copy-start.1
  196.2 0.9 copy-done.1
  197.1 19.8 %shard_map.56 = bf16[64,4096]{1,0:T(8,128)(2,1)S(1)} custom-call(bf16[256,256]{1,0:T(8,128)(2,1)S(1)} %copy-done.1, bf16[256,4096]{1,0:T(8,128)(2,1)S(1)} %copy-done), custom_call_target="tpu_custom_call" | custom-call | tf_op jit(solution)/shard_map/pallas_call | solution.py:392
  216.9 0.8 copy.10
  (6 shorter events, 0.1 us)
Async XLA Ops:
  6.5 188.1 %all-gather.2.cloned.1.call-start = ((), (), s32[]{:S(2)}) async-start(), calls=%async_computation | async-start | bytes 2359296 | tf_op jit(solution)/shard_map/all_gather | solution.py:415
  194.6 1.6 copy-start
  196.2 0.9 copy-start.1
Sparse Core Ops, SparseCore 0:
  9.4 119.3 all-gather.1
